TPU v7x, 32 devices: a whole 2x2x4 slice. The times are simulated.
32 devices in a mesh: sp: 8 (over z, x), tp: 4 (over y, core).
Axes of the slice: x: 2, y: 2, z: 4, core: 2. Of those that a mesh axis runs over, the one named last changes fastest.
Arguments:
- latent: bfloat16 [4096, 2048], P('sp'), may hold values from -6 to 6
- context: bfloat16 [512, 2048], P('sp'), may hold values from -6 to 6
- condition: bfloat16 [2048], replicated, may hold values from -6 to 6
- context_condition: bfloat16 [2048], replicated, may hold values from -6 to 6
- shift_weight: bfloat16 [2048, 2048], P('sp', 'tp'), may hold values from -0.125 to 0.125
- scale_weight: bfloat16 [2048, 2048], P('sp', 'tp'), may hold values from -0.125 to 0.125
- mod_gate_weight: bfloat16 [2048, 2048], P('sp', 'tp'), may hold values from -0.5 to 0.5
- norm_gain: bfloat16 [2048], replicated, may hold values from 0.099609375 to 1.8984375
- query_weight: bfloat16 [2048, 2048], P(None, 'tp'), may hold values from -0.125 to 0.125
- key_weight: bfloat16 [2048, 2048], P(None, 'tp'), may hold values from -0.125 to 0.125
- value_weight: bfloat16 [2048, 2048], P(None, 'tp'), may hold values from -0.125 to 0.125
- gate_weight: bfloat16 [2048, 2048], P(None, 'tp'), may hold values from -0.125 to 0.125
- forward_decay: float32 [16], P('tp'), may hold values from 0 to 1, as said below
- backward_decay: float32 [16], P('tp'), may hold values from 0 to 1, as said below
- out_weight: bfloat16 [2048, 2048], P('tp'), may hold values from -0.125 to 0.125
Outputs:
- mixed: bfloat16 [4096, 2048], P('sp')
Inputs may be any that keep to these rules, and one draw needn't show every extreme that they name: `forward_decay`: each head's rate is positive. `backward_decay`: each head's rate is positive.
All inputs are finite; a program needn't handle non-finite values.
Results may differ from a plain program's by a relative error of at most 0.015.
Values may be sent and summed in bfloat16 or wider, within the bound.
A program may use at most 64 MiB of HBM per device.

v0:
```python
import jax
import jax.numpy as jnp
from jax import lax
from jax.sharding import PartitionSpec as P

HEAD_DIM = 128
GRID_W = 64


EPS = 1e-06
THETA = 10000.0
CONTEXT_LIFT = 3.0
TOP_PRECISION = lax.Precision.HIGHEST


def carried_in(part, axis, combine, identity, reverse):
    count = lax.axis_size(axis)
    place = lax.axis_index(axis)
    ahead = count - 1 - place if reverse else place
    gathered = jax.tree.map(lambda a: lax.all_gather(a, axis), part)
    state = jax.tree.map(lambda a, e: jnp.zeros_like(a) + jnp.asarray(e, a.dtype), part, identity)

    def one(lap, state):
        source = count - 1 - lap if reverse else lap
        return combine(
            state, jax.tree.map(lambda a: lax.dynamic_index_in_dim(a, source, 0, False), gathered)
        )

    return lax.fori_loop(0, ahead, one, state)


def modulated(token_rows, norm_gain, shifts, scales):
    values = token_rows.astype(jnp.float32)
    values = values * lax.rsqrt(jnp.mean(values * values, axis=-1, keepdims=True) + EPS)
    values = values * norm_gain.astype(jnp.float32)
    return (values * (1.0 + scales) + shifts).astype(jnp.bfloat16)


def rope_half(portion, positions):
    quarter = portion.shape[-1] // 2
    frequency = THETA ** (-jnp.arange(quarter, dtype=jnp.float32) / quarter)
    angles = positions[:, None, None] * frequency
    cosine = jnp.cos(angles)
    sine_table = jnp.sin(angles)
    leading = portion[..., :quarter]
    trailing = portion[..., quarter:]
    return jnp.concatenate(
        [leading * cosine - trailing * sine_table, leading * sine_table + trailing * cosine],
        axis=-1,
    )


def rotate(values, grid_row, grid_column):
    half_width = values.shape[-1] // 2
    return jnp.concatenate(
        [
            rope_half(values[..., :half_width], grid_row),
            rope_half(values[..., half_width:], grid_column),
        ],
        axis=-1,
    )


def combine(earlier, later):
    return (earlier[0] * later[0], later[0][:, None, None] * earlier[1] + later[1])


def local(
    latent,
    context,
    condition,
    context_condition,
    shift_weight,
    scale_weight,
    mod_gate_weight,
    norm_gain,
    query_weight,
    key_weight,
    value_weight,
    gate_weight,
    forward_decay,
    backward_decay,
    out_weight,
):
    sp_index = lax.axis_index("sp")
    tp_index = lax.axis_index("tp")
    sp_count = lax.axis_size("sp")
    tp_count = lax.axis_size("tp")
    model_width = latent.shape[1]
    tokens_here = latent.shape[0]
    mod_rows = shift_weight.shape[0]
    activation = jax.nn.silu(jnp.stack([condition, context_condition]).astype(jnp.float32)).astype(
        jnp.bfloat16
    )
    own_part = lax.dynamic_slice_in_dim(activation, sp_index * mod_rows, mod_rows, 1)
    partial_value = jnp.stack(
        [
            jnp.dot(own_part, matrix, preferred_element_type=jnp.float32)
            for matrix in (shift_weight, scale_weight, mod_gate_weight)
        ]
    )
    summed = lax.psum(partial_value, "sp")
    modulation = lax.all_gather(summed, "tp", axis=2, tiled=True)
    hidden = modulated(latent, norm_gain, modulation[0, 0], modulation[1, 0])
    context_hidden = modulated(context, norm_gain, modulation[0, 1], modulation[1, 1])
    local_width = query_weight.shape[1]
    head_count = local_width // HEAD_DIM
    stacked = jnp.concatenate([query_weight, key_weight, value_weight, gate_weight], axis=1)
    projected = jnp.dot(hidden, stacked, preferred_element_type=jnp.float32).astype(jnp.bfloat16)
    queries = projected[:, :local_width]
    keys_out = projected[:, local_width : 2 * local_width]
    values_out = projected[:, 2 * local_width : 3 * local_width]
    out_gates = projected[:, 3 * local_width :]
    context_pairs = jnp.dot(
        context_hidden,
        stacked[:, local_width : 3 * local_width],
        preferred_element_type=jnp.float32,
    ).astype(jnp.bfloat16)

    def to_heads(values):
        return values.astype(jnp.float32).reshape(values.shape[0], head_count, HEAD_DIM)

    positions = sp_index * tokens_here + jnp.arange(tokens_here, dtype=jnp.int32)
    grid_row = (positions // GRID_W).astype(jnp.float32)
    grid_column = (positions % GRID_W).astype(jnp.float32)
    key_scale = HEAD_DIM ** (-0.5)
    query_heads = jnp.transpose(rotate(to_heads(queries), grid_row, grid_column), (1, 0, 2))
    key_heads = (
        jnp.transpose(rotate(to_heads(keys_out), grid_row, grid_column), (1, 0, 2)) * key_scale
    )
    value_heads = jnp.transpose(to_heads(values_out), (1, 0, 2))
    log_forward = -forward_decay
    log_backward = -backward_decay
    context_rows = context.shape[0]
    context_total = context_rows * sp_count
    context_index = (sp_index * context_rows + jnp.arange(context_rows, dtype=jnp.int32)).astype(
        jnp.float32
    )
    weight_forward = jnp.exp(log_forward[:, None] * (context_total - 1.0 - context_index)[None, :])
    weight_backward = jnp.exp(log_backward[:, None] * context_index[None, :])
    context_key_heads = to_heads(context_pairs[:, :local_width]) * (key_scale * CONTEXT_LIFT)
    context_value_heads = to_heads(context_pairs[:, local_width:])
    context_forward = jnp.einsum(
        "hc,chd,che->hde",
        weight_forward,
        context_key_heads,
        context_value_heads,
        precision=TOP_PRECISION,
    )
    context_backward = jnp.einsum(
        "hc,chd,che->hde",
        weight_backward,
        context_key_heads,
        context_value_heads,
        precision=TOP_PRECISION,
    )
    context_forward, context_backward = lax.psum((context_forward, context_backward), "sp")
    offsets = jnp.arange(tokens_here, dtype=jnp.float32)
    distance = offsets[:, None] - offsets[None, :]
    mixing = jnp.where(
        distance >= 0, jnp.exp(log_forward[:, None, None] * jnp.maximum(distance, 0.0)), 0.0
    )
    mixing = mixing + jnp.where(
        distance <= 0, jnp.exp(log_backward[:, None, None] * jnp.maximum(-distance, 0.0)), 0.0
    )
    score_matrix = (
        jnp.einsum("htd,hsd->hts", query_heads, key_heads, precision=TOP_PRECISION) * mixing
    )
    local_out = jnp.einsum("hts,hse->hte", score_matrix, value_heads, precision=TOP_PRECISION)
    tail_forward = jnp.exp(log_forward[:, None] * (tokens_here - 1.0 - offsets)[None, :])
    head_backward = jnp.exp(log_backward[:, None] * offsets[None, :])
    own_forward = jnp.einsum(
        "ht,htd,hte->hde", tail_forward, key_heads, value_heads, precision=TOP_PRECISION
    )
    own_backward = jnp.einsum(
        "ht,htd,hte->hde", head_backward, key_heads, value_heads, precision=TOP_PRECISION
    )
    span_forward = jnp.exp(log_forward * tokens_here)
    span_backward = jnp.exp(log_backward * tokens_here)
    identity = (jnp.ones_like(span_forward), jnp.zeros_like(own_forward))
    before = carried_in((span_forward, own_forward), "sp", combine, identity, False)
    after = carried_in((span_backward, own_backward), "sp", combine, identity, True)
    device_start = (sp_index * tokens_here).astype(jnp.float32)
    device_rest = ((sp_count - 1 - sp_index) * tokens_here).astype(jnp.float32)
    incoming_forward = (
        before[1] + jnp.exp(log_forward * device_start)[:, None, None] * context_forward
    )
    incoming_backward = (
        after[1] + jnp.exp(log_backward * device_rest)[:, None, None] * context_backward
    )
    read_forward = jnp.exp(log_forward[:, None] * (offsets + 1.0)[None, :])[
        :, :, None
    ] * jnp.einsum("htd,hde->hte", query_heads, incoming_forward, precision=TOP_PRECISION)
    read_backward = jnp.exp(log_backward[:, None] * (tokens_here - offsets)[None, :])[
        :, :, None
    ] * jnp.einsum("htd,hde->hte", query_heads, incoming_backward, precision=TOP_PRECISION)
    retained = local_out + read_forward + read_backward
    retained = retained * lax.rsqrt(jnp.mean(retained * retained, axis=-1, keepdims=True) + EPS)
    merged = jnp.transpose(retained, (1, 0, 2)).reshape(tokens_here, local_width)
    heads_out = (jax.nn.silu(out_gates.astype(jnp.float32)) * merged).astype(jnp.bfloat16)
    column_width = model_width // tp_count
    column_block = lax.all_to_all(out_weight, "tp", split_axis=1, concat_axis=0, tiled=True)
    projection = jnp.dot(
        lax.all_gather(heads_out, "tp", axis=1, tiled=True),
        column_block,
        preferred_element_type=jnp.float32,
    )
    own_latent = lax.dynamic_slice_in_dim(latent, tp_index * column_width, column_width, 1)
    own_gate = lax.dynamic_slice_in_dim(modulation[2, 0], tp_index * column_width, column_width, 0)
    finished = (own_latent.astype(jnp.float32) + own_gate * projection).astype(jnp.bfloat16)
    return lax.all_gather(finished, "tp", axis=1, tiled=True)


def solution(mesh):
    placed = (
        P("sp", None),
        P("sp", None),
        P(),
        P(),
        P("sp", "tp"),
        P("sp", "tp"),
        P("sp", "tp"),
        P(),
        P(None, "tp"),
        P(None, "tp"),
        P(None, "tp"),
        P(None, "tp"),
        P("tp"),
        P("tp"),
        P("tp", None),
    )
    return jax.shard_map(
        local, mesh=mesh, in_specs=placed, out_specs=P("sp", None), check_vma=False
    )
```

profile of v0, /device:TPU:0, one launch (start us, length us, event | category | flops | bytes accessed | tf_op | source)
XLA Modules:
  0.0 348.2 jit_solution(2513971248840117327)
XLA Ops:
  13.8 38.8 %all-reduce.2 = (f32[3,2,512]{2,1,0:T(2,128)S(1)}, f32[32]{0:T(128)S(1)}, f32[32]{0:T(128)S(1)}) all-reduce(f32[3,2,512]{2,1,0:T(2,128)S(1)} %pad_maximum_fusion, f32[32]{0:T(128)S(1)} %get-tuple-element.202, f32[32]{0:T(128)S(1)} %get-tuple-element.199), channel_id=1, replica_groups=mesh['sp'=8,'tp'=4] {'sp'}, use_global_device_ids=true, to_apply=%region_0.1 | all-reduce | flops 3136 | bytes 25088 | tf_op jit(solution)/shard_map/psum | solution.py:102
  52.6 5.2 %all_gather.33 = f32[3,2,2048]{2,1,0:T(2,128)S(1)} all-gather(f32[3,2,512]{2,1,0:T(2,128)S(1)} %get-tuple-element.155), channel_id=1, replica_groups=mesh['sp'=8,'tp'=4] {'tp'}, dimensions={2}, use_global_device_ids=true | all-gather | bytes 61440 | tf_op jit(solution)/shard_map/all_gather | solution.py:103
  58.6 2.1 fusion.8
  60.6 10.4 %fusion.26 = bf16[512,2048]{1,0:T(8,128)(2,1)S(1)} fusion(bf16[2048,512]{1,0:T(8,128)(2,1)} %param.30, bf16[2048,512]{1,0:T(8,128)(2,1)} %param.29, bf16[2048,512]{1,0:T(8,128)(2,1)} %param.28, bf16[2048,512]{1,0:T(8,128)(2,1)} %param.27, bf16[512,2048]{1,0:T(8,128)(2,1)} %param.19, f32[2048]{0:T(1024)S(1)} %bitcast.97, f32[2048]{0:T(1024)S(1)} %bitcast.98, ...), kind=kOutput, calls=%fused_computation.32 | convolution fusion | flops 4335861760 | bytes 12609536 | tf_op jit(solution)/shard_map/dot_general | solution.py:109
  74.9 3.4 fusion.107
  86.8 2.0 fusion.55
  89.2 3.2 fusion.43
  97.2 3.1 maximum_bitcast_fusion
  100.3 4.9 %fusion.60 = f32[4,512,512]{2,1,0:T(8,128)} fusion(f32[4,512,128]{2,1,0:T(8,128)S(1)} %maximum_bitcast_fusion, f32[4,512,128]{2,1,0:T(8,128)S(1)} %maximum_bitcast_fusion.1), kind=kOutput, calls=%fused_computation.74 | convolution fusion | flops 1610874880 | bytes 6291456 | tf_op jit(solution)/shard_map/htd,hsd->hts/dot_general | solution.py:167
  105.4 7.0 %fusion.17 = f32[4,512,128]{1,2,0:T(8,128)S(1)} fusion(bf16[4,512,128]{1,2,0:T(8,128)(2,1)S(1)} %bitcast.90, f32[4,512,512]{2,1,0:T(8,128)} %fusion.60, f32[512,512]{1,0:T(8,128)} %get-tuple-element.214, f32[4]{0:T(128)S(1)} %get-tuple-element.203, f32[512,512]{1,0:T(8,128)} %get-tuple-element.215, f32[4]{0:T(128)S(1)} %get-tuple-element.200, ...), kind=kOutput, calls=%fused_computation.23 | convolution fusion | flops 1616904192 | bytes 8388640 | tf_op jit(solution)/shard_map/hts,hse->hte/dot_general | solution.py:169
  112.4 20.9 %all-gather.15.cloned.1.call-done = f32[32,128,128]{2,1,0:T(8,128)} async-done(((f32[4,128,128]{2,1,0:T(8,128)}), f32[32,128,128]{2,1,0:T(8,128)}) %all-gather.15.cloned.1.call-update) | async-done | bytes 2097168 | tf_op jit(solution)/shard_map/all_gather | solution.py:20
  133.3 7.7 %while.27 = (s32[]{:T(128)}, f32[4,128,128]{2,1,0:T(8,128)S(1)}, s32[]{:T(128)}, f32[8,4]{1,0:T(8,128)S(1)}, f32[8,4,128,128]{3,2,1,0:T(8,128)}, /*index=5*/s32[]{:T(128)}, s32[]{:T(128)}, s32[]{:T(128)}, s32[]{:T(128)}) while((s32[]{:T(128)}, f32[4,128,128]{2,1,0:T(8,128)S(1)}, s32[]{:T(128)}, f32[8,4]{1,0:T(8,128)S(1)}, ...), condition=%wide.region_7.8_spmd, body=%wide.region_6.7_spmd.sunk | while | flops 131078 | bytes 786635 | solution.py:29
  141.0 42.1 %all-gather.13.cloned.1.call-done = f32[32,128,128]{2,1,0:T(8,128)} async-done(((f32[4,128,128]{2,1,0:T(8,128)}), f32[32,128,128]{2,1,0:T(8,128)}) %all-gather.13.cloned.1.call-update) | async-done | bytes 2097168 | tf_op jit(solution)/shard_map/all_gather | solution.py:20
  183.2 74.8 %all-reduce.6.cloned.1.call-done = (f32[4,128,128]{2,1,0:T(8,128)}, f32[4,128,128]{2,1,0:T(8,128)}) async-done(((f32[4,128,128]{2,1,0:T(8,128)}, f32[4,128,128]{2,1,0:T(8,128)}), (f32[4,128,128]{2,1,0:T(8,128)}, f32[4,128,128]{2,1,0:T(8,128)})) %all-reduce.6.cloned.1.call-update) | async-done | bytes 524304 | tf_op jit(solution)/shard_map/psum | solution.py:157
  258.0 2.1 fusion.75
  260.1 2.3 multiply_reduce_fusion
  265.6 2.2 fusion.62
  267.8 2.5 copy.90
  270.3 3.6 %all-to-all-start = ((bf16[512,4,512]{0,2,1:T(8,128)(2,1)}), bf16[512,4,512]{0,2,1:T(8,128)(2,1)S(1)}, u32[]{:S(2)}, u32[]{:S(2)}) async-start(bf16[512,4,512]{0,2,1:T(8,128)(2,1)} %bitcast.87), calls=%async_computation | async-start | bytes 4194304 | tf_op jit(solution)/shard_map/all_to_all | solution.py:202
  274.0 36.6 %all-to-all-done = bf16[512,4,512]{0,2,1:T(8,128)(2,1)S(1)} async-done(((bf16[512,4,512]{0,2,1:T(8,128)(2,1)}), bf16[512,4,512]{0,2,1:T(8,128)(2,1)S(1)}, u32[]{:S(2)}, u32[]{:S(2)}) %all-to-all-start) | async-done | bytes 2097184 | tf_op jit(solution)/shard_map/all_to_all | solution.py:202
  310.6 2.4 copy.91
  313.0 4.4 %fusion.42 = bf16[512,512]{1,0:T(8,128)(2,1)} fusion(bf16[512,2048]{1,0:T(8,128)(2,1)} %all-gather.9.cloned.1.call-done, bf16[2048,512]{1,0:T(8,128)(2,1)} %bitcast.92, f32[512]{0:T(512)S(1)} %bitcast.99, bf16[512,2048]{1,0:T(8,128)(2,1)} %param.19, s32[]{:T(128)S(6)} %select_n.51), kind=kOutput, calls=%fused_computation.48 | convolution fusion | flops 1074790400 | bytes 5244932 | tf_op jit(solution)/shard_map/dot_general | solution.py:203
  317.4 21.2 %all-gather.11.cloned.1.call-done = bf16[512,2048]{1,0:T(8,128)(2,1)} async-done(((bf16[512,512]{1,0:T(8,128)(2,1)}), bf16[512,2048]{1,0:T(8,128)(2,1)}) %all-gather.11.cloned.1.call-update) | async-done | bytes 2097168 | tf_op jit(solution)/shard_map/all_gather | solution.py:211
  338.5 3.2 copy.159
  (86 shorter events, 35.6 us)
Async XLA Ops:
  6.5 1.5 copy-start
  6.5 126.7 %all-gather.15.cloned.1.call-start = ((), (), s32[]{:S(2)}) async-start(), calls=%async_computation.4 | async-start | bytes 2359296 | tf_op jit(solution)/shard_map/all_gather | solution.py:20
  71.1 1.7 copy-start.3
  83.7 5.2 %copy-start.4 = (bf16[64,2048]{1,0:T(8,128)(2,1)S(1)}, bf16[64,2048]{1,0:T(8,128)(2,1)}, u32[]{:S(2)}) copy-start(bf16[64,2048]{1,0:T(8,128)(2,1)} %param.20) | copy-start | bytes 786436
  86.7 96.4 %all-gather.13.cloned.1.call-start = ((), (), s32[]{:S(2)}) async-start(), calls=%async_computation.3 | async-start | bytes 2359296 | tf_op jit(solution)/shard_map/all_gather | solution.py:20
  88.8 169.2 %all-reduce.6.cloned.1.call-start = ((), (), s32[]{:S(2)}) async-start(), calls=%async_computation.5 | async-start | bytes 1048576 | tf_op jit(solution)/shard_map/psum | solution.py:157
  94.8 218.2 %all-gather.9.cloned.1.call-start = ((), (), s32[]{:S(2)}) async-start(), calls=%async_computation.1 | async-start | bytes 2621440 | tf_op jit(solution)/shard_map/all_gather | solution.py:204
  263.8 3.9 %copy-start.2 = (bf16[512,2048]{1,0:T(8,128)(2,1)S(1)}, bf16[512,2048]{1,0:T(8,128)(2,1)}, u32[]{:S(2)}) copy-start(bf16[512,2048]{1,0:T(8,128)(2,1)} %param.33) | copy-start | bytes 6291460
  270.3 40.3 %all-to-all-start = ((bf16[512,4,512]{0,2,1:T(8,128)(2,1)}), bf16[512,4,512]{0,2,1:T(8,128)(2,1)S(1)}, u32[]{:S(2)}, u32[]{:S(2)}) async-start(bf16[512,4,512]{0,2,1:T(8,128)(2,1)} %bitcast.87), calls=%async_computation | async-start | bytes 4194304 | tf_op jit(solution)/shard_map/all_to_all | solution.py:202
  273.9 64.6 %all-gather.11.cloned.1.call-start = ((), (), s32[]{:S(2)}) async-start(), calls=%async_computation.2 | async-start | bytes 2621440 | tf_op jit(solution)/shard_map/all_gather | solution.py:211
  313.0 28.7 %copy-start.1 = (bf16[256,512]{1,0:T(8,128)(2,1)S(1)}, bf16[256,512]{1,0:T(8,128)(2,1)}, u32[]{:S(2)}) copy-start(bf16[256,512]{1,0:T(8,128)(2,1)} %param.25) | copy-start | bytes 786436
Sparse Core Ops, SparseCore 0:
  86.8 46.4 all-gather.14
  135.4 47.6 all-gather.12
  186.6 71.3 all-reduce.5
  267.9 33.0 all-gather.8
  317.5 20.9 all-gather.10
where the time goes:
time: 349 us; the launch traced here: 348 us
  waiting for transfers between devices  196 us (56%)
  blocking collectives  44 us (13%)
  matrix products  43.1 us (12%)
  other arithmetic  29 us (8%)
  local copies, waits for them, and re-layouts  18.2 us (5%)
  between operations  14.1 us (4%)
  starting transfers between devices  4.03 us (1%)
    psum x1, waiting for transfers between devices, local(): lax.psum((context_forward, context_backward), 'sp')  74.8 us
    all_gather x2, waiting for transfers between devices, carried_in(): gathered = jax.tree.map(lambda a: lax.all_gather(a, axis), part)  63 us
    psum x1, blocking collectives, local(): summed = lax.psum(partial_value, 'sp')  38.8 us
    all_to_all x1, waiting for transfers between devices, local(): lax.all_to_all(out_weight, 'tp', split_axis=1, concat_axis=0, tiled=True)  36.6 us
    all_gather x1, waiting for transfers between devices, local(): return lax.all_gather(finished, 'tp', axis=1, tiled=True)  21.2 us
    dot_general x1, matrix products, local(): jnp.dot(hidden, stacked, preferred_element_type=jnp.float32)  10.4 us
    add x7, other arithmetic, combine(): later[0][:, None, None] * earlier[1] + later[1]  7.43 us
    unnamed x15, local copies, waits for them, and re-layouts  6.99 us
  transfers between devices with their start and end apart: 6, of which 5 were waited for; matrix products, arithmetic and copies ran while one was open for 11% of the time, Pallas kernels for 0%

commit v1 on v0

v1 whole, which is shorter than its diff:
```python
import functools
import math

import jax
import jax.numpy as jnp
from jax import lax
from jax.experimental import pallas as pl
from jax.experimental.pallas import tpu as pltpu
from jax.sharding import PartitionSpec as P

HEAD_DIM = 128
GRID_W = 64
EPS = 1e-06
THETA = 10000.0
CONTEXT_LIFT = 3.0
MESH = pl.DeviceIdType.MESH
F32 = jnp.float32
BF16 = jnp.bfloat16


def dot(a, b):
    return jnp.dot(a, b, preferred_element_type=F32)


def dot_rows(a, b):
    return lax.dot_general(a, b, (((0,), (0,)), ((), ())), preferred_element_type=F32)


def dot_columns(a, b):
    return lax.dot_general(a, b, (((1,), (1,)), ((), ())), preferred_element_type=F32)


def rotated(x, cosines, sines, low):
    partner = jnp.where(low, pltpu.roll(x, HEAD_DIM - 32, 1), pltpu.roll(x, 32, 1))
    return x * cosines + partner * sines


def kernel(
    sp_n,
    tp_n,
    act,
    gain,
    fd,
    bd,
    latent_h,
    context_h,
    shift_h,
    scale_h,
    gate_h,
    wq_h,
    wk_h,
    wv_h,
    wg_h,
    ow_h,
    out_h,
    lat,
    ctx,
    modw,
    wbuf,
    hid,
    mod_part,
    mod_recv,
    mod_sum,
    mod_all,
    inv,
    cosb,
    sinb,
    proj,
    mix,
    local,
    heads_all,
    ow_all,
    acc,
    out_v,
    sc_send,
    sc_recv,
    sl_send,
    sl_recv,
    in_send,
    in_recv,
    load_sem,
    m1s,
    m1r,
    m2s,
    m2r,
    scs,
    scr,
    sls,
    slr,
    ins,
    inr,
    wys,
    wyr,
    wps,
    wpr,
    hys,
    hyr,
    hps,
    hpr,
    out_sem,
):
    me = lax.axis_index("sp")
    tp = lax.axis_index("tp")
    y_n = tp_n // 2
    my_y = tp // 2
    core = lax.rem(tp, 2)
    other = my_y * 2 + 1 - core
    T, D = lat.shape
    CR = ctx.shape[0]
    W = wbuf.shape[2]
    H = W // HEAD_DIM
    R = sl_send.shape[1]
    per = HEAD_DIM // R

    loads = [
        pltpu.make_async_copy(src, dst, load_sem.at[i])
        for i, (src, dst) in enumerate(
            [
                (shift_h, modw.at[0]),
                (scale_h, modw.at[1]),
                (gate_h, modw.at[2]),
                (latent_h, lat),
                (context_h, ctx),
                (wk_h, wbuf.at[1]),
                (wv_h, wbuf.at[2]),
                (wq_h, wbuf.at[0]),
                (wg_h, wbuf.at[3]),
                (ow_h, ow_all.at[pl.ds(tp * H, H)]),
            ]
        )
    ]
    for load in loads:
        load.start()

    barrier = pltpu.get_barrier_semaphore()

    def greet(axis, mine, n):
        def one(off, carry):
            pl.semaphore_signal(
                barrier, inc=1, device_id={axis: lax.rem(mine + off, n)}, device_id_type=MESH
            )
            return carry

        lax.fori_loop(1, n, one, 0)

    greet("sp", me, sp_n)
    greet("tp", tp, tp_n)

    def remote(src, dst, ss, rs, where):
        return pltpu.make_async_remote_copy(
            src_ref=src,
            dst_ref=dst,
            send_sem=ss,
            recv_sem=rs,
            device_id=where,
            device_id_type=MESH,
        )

    def each(n, body):
        def one(off, carry):
            body(off)
            return carry

        lax.fori_loop(1, n, one, 0)

    def sp_copy(off, src, dst, ss, rs):
        return remote(src, dst, ss.at[off], rs.at[off], {"sp": lax.rem(me + off, sp_n)})

    a = act[me].astype(F32)
    activation = (a / (1.0 + jnp.exp(-a))).astype(BF16)
    for i in range(3):
        loads[i].wait()
        mod_part[2 * i : 2 * i + 2, :] = dot(activation, modw[i])[0:2, :]
    mod_part[6:8, :] = jnp.zeros((2, W), F32)
    pl.semaphore_wait(barrier, sp_n - 1 + tp_n - 1)

    def m1(off):
        return sp_copy(off, mod_part, mod_recv.at[me], m1s, m1r)

    each(sp_n, lambda off: m1(off).start())

    def y_peer(off):
        return {"tp": lax.rem(my_y + off, y_n) * 2 + core}

    def y_source(off):
        return lax.rem(my_y - off + y_n, y_n) * 2 + core

    def wy(off, c):
        return remote(
            ow_h.at[c],
            ow_all.at[tp * H + c],
            wys.at[off * H + c],
            wyr.at[off * H + c],
            y_peer(off),
        )

    def wp(off, c):
        block = y_source(off) * H + c
        return remote(
            ow_all.at[block],
            ow_all.at[block],
            wps.at[off * H + c],
            wpr.at[off * H + c],
            {"tp": other},
        )

    for c in range(H):
        each(y_n, lambda off: wy(off, c).start())

    def relay_weight(c):
        def one(off):
            wy(off, c).wait_recv()
            wp(off, c).start()

        each(y_n, one)

    rows = 64
    loads[3].wait()
    loads[4].wait()

    def stat(source, base):
        height = min(rows, source.shape[0])

        def one(i, carry):
            r = pl.multiple_of(i * height, height)
            x = source[pl.ds(r, height), :].astype(F32)
            mean = jnp.mean(x * x, axis=-1, keepdims=True)
            inv[pl.ds(pl.multiple_of(base + r, height), height), :] = jnp.broadcast_to(
                lax.rsqrt(mean + EPS), (height, HEAD_DIM)
            )
            return carry

        lax.fori_loop(0, source.shape[0] // height, one, 0)

    stat(lat, 0)
    stat(ctx, T)

    each(sp_n, lambda off: m1(off).wait_recv())
    mod_recv[me] = mod_part[...]
    mod_sum[...] = lax.fori_loop(
        0, sp_n, lambda s, total: total + mod_recv[s], jnp.zeros((8, W), F32)
    )

    def m2(off):
        return remote(
            mod_sum,
            mod_all.at[tp],
            m2s.at[off],
            m2r.at[off],
            {"tp": lax.rem(tp + off, tp_n)},
        )

    each(tp_n, lambda off: m2(off).start())
    mod_all[tp] = mod_sum[...]
    loads[9].wait()

    def wown(c):
        block = tp * H + c
        return remote(
            ow_all.at[block], ow_all.at[block], wps.at[c], wpr.at[c], {"tp": other}
        )

    for c in range(H):
        wown(c).start()

    token = lax.broadcasted_iota(jnp.int32, (T, HEAD_DIM), 0)
    lane = lax.broadcasted_iota(jnp.int32, (T, HEAD_DIM), 1)
    place = me * T + token
    spot = jnp.where(lane < 64, place >> 6, place & 63).astype(F32)
    angle = spot * jnp.exp((lane & 31).astype(F32) * (-math.log(THETA) / 32.0))
    cosb[...] = jnp.cos(angle)
    sine = jnp.sin(angle)
    sinb[...] = jnp.where((lane & 32) == 0, -sine, sine)

    mt = 128

    def mix_rows(i, carry):
        r = pl.multiple_of(i * mt, mt)
        gap = (
            i * mt
            + lax.broadcasted_iota(jnp.int32, (mt, T), 0)
            - lax.broadcasted_iota(jnp.int32, (mt, T), 1)
        )
        gapf = gap.astype(F32)
        for h in range(H):
            weight = jnp.exp(jnp.where(gap >= 0, -fd[h] * gapf, bd[h] * gapf))
            mix[h, pl.ds(r, mt), :] = jnp.where(gap == 0, 2.0, weight).astype(BF16)
        return carry

    lax.fori_loop(0, T // mt, mix_rows, 0)

    each(tp_n, lambda off: m2(off).wait_recv())

    def modulate(source, base, row):
        height = min(rows, source.shape[0])
        tiles = source.shape[0] // height

        def one(i, carry):
            b = i // tiles
            r = pl.multiple_of(lax.rem(i, tiles) * height, height)
            cols = pl.ds(pl.multiple_of(b * W, W), W)
            out_rows = pl.ds(pl.multiple_of(base + r, height), height)
            x = source[pl.ds(r, height), cols].astype(F32) * inv[out_rows, 0:1]
            x = x * gain[:, cols]
            x = x * (1.0 + mod_all[b, 2 + row : 3 + row, :]) + mod_all[b, row : row + 1, :]
            hid[out_rows, cols] = x.astype(BF16)
            return carry

        lax.fori_loop(0, tp_n * tiles, one, 0)

    modulate(lat, 0, 0)
    modulate(ctx, T, 1)

    nt = min(256, W)

    def project(index, height):
        def one(j, carry):
            cols = pl.ds(pl.multiple_of(j * nt, nt), nt)
            proj[index, 0:height, cols] = dot(hid[0:height, :], wbuf[index, :, cols]).astype(BF16)
            return carry

        lax.fori_loop(0, W // nt, one, 0)

    loads[5].wait()
    project(1, T + CR)
    loads[6].wait()
    project(2, T + CR)

    scale = HEAD_DIM**-0.5
    step = token.astype(F32)
    low = (lane & 32) == 0
    cpos = (me * CR + lax.broadcasted_iota(jnp.int32, (CR, HEAD_DIM), 0)).astype(F32)
    ctotal = float(CR * sp_n)

    def put(ref, d, h, value):
        start = (d * H + h) * per
        ref[start : start + per] = value.reshape(per, R, HEAD_DIM).astype(BF16)

    for h in range(H):
        cols = slice(h * HEAD_DIM, (h + 1) * HEAD_DIM)
        ck = proj[1, T : T + CR, cols].astype(F32) * (scale * CONTEXT_LIFT)
        cv = proj[2, T : T + CR, cols]
        put(sc_send, 0, h, dot_rows((ck * jnp.exp(-fd[h] * (ctotal - 1.0 - cpos))).astype(BF16), cv))
        put(sc_send, 1, h, dot_rows((ck * jnp.exp(-bd[h] * cpos)).astype(BF16), cv))

    def scopy(off):
        return sp_copy(off, sc_send.at[lax.rem(me + off, sp_n)], sc_recv.at[me], scs, scr)

    def slcopy(off):
        return sp_copy(off, sl_send.at[lax.rem(me + off, sp_n)], sl_recv.at[me], sls, slr)

    def incopy(off):
        return sp_copy(off, in_send.at[lax.rem(me + off, sp_n)], in_recv.at[me], ins, inr)

    each(sp_n, lambda off: scopy(off).start())

    for h in range(H):
        cols = slice(h * HEAD_DIM, (h + 1) * HEAD_DIM)
        k = rotated(proj[1, 0:T, cols].astype(F32), cosb[...], sinb[...], low) * scale
        v = proj[2, 0:T, cols]
        put(sl_send, 0, h, dot_rows((k * jnp.exp(-fd[h] * (T - 1.0 - step))).astype(BF16), v))
        put(sl_send, 1, h, dot_rows((k * jnp.exp(-bd[h] * step)).astype(BF16), v))
        proj[1, 0:T, cols] = k.astype(BF16)

    each(sp_n, lambda off: slcopy(off).start())
    sc_recv[me] = sc_send[me]
    sl_recv[me] = sl_send[me]

    loads[7].wait()
    project(0, T)
    loads[8].wait()
    project(3, T)

    each(sp_n, lambda off: scopy(off).wait_recv())
    each(sp_n, lambda off: slcopy(off).wait_recv())
    backward = (me * R) // (H * HEAD_DIM)
    head = lax.rem((me * R) // HEAD_DIM, H)
    rate = jnp.where(backward == 1, bd[head], fd[head])
    span = jnp.exp(jnp.full((R, HEAD_DIM), -float(T), F32) * rate)
    start = lax.fori_loop(
        0, sp_n, lambda s, total: total + sc_recv[s].astype(F32), jnp.zeros((R, HEAD_DIM), F32)
    )

    def scan(lap, state):
        i = jnp.where(backward == 1, sp_n - 1 - lap, lap)
        in_send[i] = state.astype(BF16)
        return span * state + sl_recv[i].astype(F32)

    lax.fori_loop(0, sp_n, scan, start)
    each(sp_n, lambda off: incopy(off).start())
    in_recv[me] = in_send[me]

    for h in range(H):
        cols = slice(h * HEAD_DIM, (h + 1) * HEAD_DIM)
        q = rotated(proj[0, 0:T, cols].astype(F32), cosb[...], sinb[...], low).astype(BF16)
        proj[0, 0:T, cols] = q

        def score_rows(i, carry):
            r = pl.ds(pl.multiple_of(i * mt, mt), mt)
            s = dot_columns(proj[0, r, cols], proj[1, 0:T, cols]) * mix[h, r, :].astype(F32)
            local[r, cols] = dot(s.astype(BF16), proj[2, 0:T, cols])
            return carry

        lax.fori_loop(0, T // mt, score_rows, 0)

    each(sp_n, lambda off: incopy(off).wait_recv())

    def hview(block, h):
        return heads_all.at[block, :, pl.ds(h * HEAD_DIM, HEAD_DIM)]

    def hy(off, h):
        return remote(
            hview(tp, h), hview(tp, h), hys.at[off * H + h], hyr.at[off * H + h], y_peer(off)
        )

    def hp(off, h):
        block = y_source(off)
        return remote(
            hview(block, h),
            hview(block, h),
            hps.at[off * H + h],
            hpr.at[off * H + h],
            {"tp": other},
        )

    def hown(h):
        return remote(hview(tp, h), hview(tp, h), hps.at[h], hpr.at[h], {"tp": other})

    for h in range(H):
        cols = slice(h * HEAD_DIM, (h + 1) * HEAD_DIM)
        q = proj[0, 0:T, cols].astype(F32)
        at = h * per
        forward = in_recv[at : at + per].astype(F32).reshape(HEAD_DIM, HEAD_DIM).astype(BF16)
        at = (H + h) * per
        back = in_recv[at : at + per].astype(F32).reshape(HEAD_DIM, HEAD_DIM).astype(BF16)
        kept = (
            local[:, cols]
            + dot((q * jnp.exp(-fd[h] * (step + 1.0))).astype(BF16), forward)
            + dot((q * jnp.exp(-bd[h] * (T - step))).astype(BF16), back)
        )
        kept = kept * lax.rsqrt(jnp.mean(kept * kept, axis=-1, keepdims=True) + EPS)
        g = proj[3, 0:T, cols].astype(F32)
        heads_all[tp, :, cols] = (g / (1.0 + jnp.exp(-g)) * kept).astype(BF16)
        each(y_n, lambda off: hy(off, h).start())
        hown(h).start()

    for c in range(H):
        relay_weight(c)

    ot = 256

    def block_product(block, first, last):
        def one(j, carry):
            cols = pl.ds(pl.multiple_of(j * ot, ot), ot)
            value = None
            for c in range(0, H, 2 if H % 2 == 0 else 1):
                width = 2 if H % 2 == 0 else 1
                piece = heads_all[block, :, c * HEAD_DIM : (c + width) * HEAD_DIM]
                weight = ow_all[pl.ds(block * H + c, width), :, cols].reshape(
                    width * HEAD_DIM, ot
                )
                term = dot(piece, weight)
                value = term if value is None else value + term
            if not first:
                value = value + acc[:, cols]
            acc[:, cols] = value
            return carry

        lax.fori_loop(0, D // ot, one, 0)

    block_product(tp, True, False)
    for h in range(H):
        hown(h).wait_recv()
        wown(h).wait_recv()
    block_product(other, False, False)

    def far(off):
        for h in range(H):
            hy(off, h).wait_recv()
            hp(off, h).start()
        block_product(y_source(off), False, False)

    each(y_n, far)

    def farther(off):
        for h in range(H):
            hp(off, h).wait_recv()
            wp(off, h).wait_recv()
        block_product(lax.rem(my_y - off + y_n, y_n) * 2 + 1 - core, False, False)

    each(y_n, farther)

    def finish(i, carry):
        b = i // (T // rows)
        r = pl.multiple_of(lax.rem(i, T // rows) * rows, rows)
        cols = pl.ds(pl.multiple_of(b * W, W), W)
        value = lat[pl.ds(r, rows), cols].astype(F32) + mod_all[b, 4:5, :] * acc[pl.ds(r, rows), cols]
        out_v[pl.ds(r, rows), cols] = value.astype(BF16)
        return carry

    lax.fori_loop(0, tp_n * (T // rows), finish, 0)
    result = pltpu.make_async_copy(out_v, out_h, out_sem)
    result.start()

    each(sp_n, lambda off: m1(off).wait_send())
    each(tp_n, lambda off: m2(off).wait_send())
    each(sp_n, lambda off: scopy(off).wait_send())
    each(sp_n, lambda off: slcopy(off).wait_send())
    each(sp_n, lambda off: incopy(off).wait_send())
    for h in range(H):
        wown(h).wait_send()
        hown(h).wait_send()

    def settle(off):
        for h in range(H):
            wy(off, h).wait_send()
            wp(off, h).wait_send()
            hy(off, h).wait_send()
            hp(off, h).wait_send()

    each(y_n, settle)
    result.wait()


def local_program(
    sp_n,
    tp_n,
    latent,
    context,
    condition,
    context_condition,
    shift_weight,
    scale_weight,
    mod_gate_weight,
    norm_gain,
    query_weight,
    key_weight,
    value_weight,
    gate_weight,
    forward_decay,
    backward_decay,
    out_weight,
):
    T, D = latent.shape
    CR = context.shape[0]
    MR, W = shift_weight.shape
    H = W // HEAD_DIM
    R = 2 * H * HEAD_DIM // sp_n
    pair = jnp.stack([condition, context_condition]).reshape(2, sp_n, MR)
    act = jnp.pad(jnp.transpose(pair, (1, 0, 2)), ((0, 0), (0, 14), (0, 0)))
    gain = norm_gain.astype(F32).reshape(1, D)
    ow = out_weight.reshape(H, HEAD_DIM, D)
    y_n = tp_n // 2
    vm = pl.BlockSpec(memory_space=pltpu.VMEM)
    sm = pl.BlockSpec(memory_space=pltpu.SMEM)
    hb = pl.BlockSpec(memory_space=pl.ANY)
    V = pltpu.VMEM
    dma = pltpu.SemaphoreType.DMA
    state = V((sp_n, R, HEAD_DIM), BF16)
    return pl.pallas_call(
        functools.partial(kernel, sp_n, tp_n),
        out_shape=jax.ShapeDtypeStruct((T, D), BF16),
        in_specs=[vm, vm, sm, sm] + [hb] * 10,
        out_specs=hb,
        scratch_shapes=[
            V((T, D), BF16),
            V((CR, D), BF16),
            V((3, MR, W), BF16),
            V((4, D, W), BF16),
            V((T + CR, D), BF16),
            V((8, W), F32),
            V((sp_n, 8, W), F32),
            V((8, W), F32),
            V((tp_n, 8, W), F32),
            V((T + CR, HEAD_DIM), F32),
            V((T, HEAD_DIM), F32),
            V((T, HEAD_DIM), F32),
            V((4, T + CR, W), BF16),
            V((H, T, T), BF16),
            V((T, W), F32),
            V((tp_n, T, W), BF16),
            V((tp_n * H, HEAD_DIM, D), BF16),
            V((T, D), F32),
            V((T, D), BF16),
            state,
            state,
            state,
            state,
            state,
            state,
            dma((10,)),
            dma((sp_n,)),
            dma((sp_n,)),
            dma((tp_n,)),
            dma((tp_n,)),
        ]
        + [dma((sp_n,))] * 6
        + [dma((y_n * H,))] * 8
        + [dma],
        compiler_params=pltpu.CompilerParams(
            collective_id=0, has_side_effects=True, vmem_limit_bytes=60 * 1024 * 1024
        ),
    )(
        act,
        gain,
        forward_decay,
        backward_decay,
        latent,
        context,
        shift_weight,
        scale_weight,
        mod_gate_weight,
        query_weight,
        key_weight,
        value_weight,
        gate_weight,
        ow,
    )


def solution(mesh):
    placed = (
        P("sp", None),
        P("sp", None),
        P(),
        P(),
        P("sp", "tp"),
        P("sp", "tp"),
        P("sp", "tp"),
        P(),
        P(None, "tp"),
        P(None, "tp"),
        P(None, "tp"),
        P(None, "tp"),
        P("tp"),
        P("tp"),
        P("tp", None),
    )
    return jax.shard_map(
        functools.partial(local_program, mesh.shape["sp"], mesh.shape["tp"]),
        mesh=mesh,
        in_specs=placed,
        out_specs=P("sp", None),
        check_vma=False,
    )
```

time: 349 us -> 106 us (0.30)
  waiting for transfers between devices: 196 us -> 0 us
  Pallas kernels: 0 us -> 99.3 us
  blocking collectives: 44 us -> 0 us
  matrix products: 43.1 us -> 0 us
  other arithmetic: 29 us -> 1.31 us
  between operations: 14.1 us -> 0.01 us
  local copies, waits for them, and re-layouts: 18.2 us -> 5.19 us
  starting transfers between devices: 4.03 us -> 0 us
    pallas_call x0 -> x1, Pallas kernels: none -> 99.3 us  [local_program(): pl.pallas_call(functools.partial(kernel, sp_n, tp_n), out_shape=jax.Shape...]
    all_gather x4 -> x0, waiting for transfers between devices: 84.1 us -> none  [the longest x2 63 us: carried_in(): gathered = jax.tree.map(lambda a: lax.all_gather(a, axis), part)]
    psum x1 -> x0, waiting for transfers between devices: 74.8 us -> none  [local(): lax.psum((context_forward, context_backward), 'sp')]
    dot_general x14 -> x0, matrix products: 43.1 us -> none  [the longest x1 10.4 us: local(): jnp.dot(hidden, stacked, preferred_element_type=jnp.float32)]
    psum x1 -> x0, blocking collectives: 38.8 us -> none  [local(): summed = lax.psum(partial_value, 'sp')]
    all_to_all x1 -> x0, waiting for transfers between devices: 36.6 us -> none  [local(): lax.all_to_all(out_weight, 'tp', split_axis=1, concat_axis=0, tiled=True)]
    add x8 -> x0, other arithmetic: 7.44 us -> none  [the longest x7 7.43 us: combine(): later[0][:, None, None] * earlier[1] + later[1]]
    all_gather x1 -> x0, blocking collectives: 5.2 us -> none  [local(): modulation = lax.all_gather(summed, 'tp', axis=2, tiled=True)]
  transfers between devices with their start and end apart: 6 -> 0, of which waited for: 5 -> 0; matrix products, arithmetic and copies ran while one was open for 11% -> 0% of each run, Pallas kernels for 0% -> 0%
where the time goes in v1:
time: 106 us
  Pallas kernels  99.3 us (94%)
  local copies, waits for them, and re-layouts  5.19 us (5%)
  other arithmetic  1.31 us (1%)
    pallas_call x1, Pallas kernels, local_program(): pl.pallas_call(functools.partial(kernel, sp_n, tp_n), out_shape=jax.Shape...  99.3 us
    unnamed x1, local copies, waits for them, and re-layouts  3.16 us

profile of v1, /device:TPU:0, one launch (start us, length us, event | category | flops | bytes accessed | tf_op | source)
XLA Modules:
  0.0 105.8 jit_solution(5009420085183716039)
XLA Ops:
  0.0 0.7 stack.12
  0.7 0.7 stack.13
  1.4 1.3 %reshape.16 = f32[2048]{0:T(1024)} convert(bf16[2048]{0:T(1024)(128)(2,1)} %param.22) | non-fusion elementwise | flops 2048 | bytes 12288 | tf_op jit(solution)/shard_map/reshape | solution.py:551
  2.7 0.6 pad.4.act
  3.3 99.3 %shard_map.145 = bf16[512,2048]{1,0:T(8,128)(2,1)} custom-call(bf16[8,16,256]{2,1,0:T(8,128)(2,1)} %pad.4.act, f32[1,2048]{1,0:T(1,128)} %bitcast.5, f32[4]{0:T(128)} %fd.1, f32[4]{0:T(128)} %bd.1, bf16[512,2048]{1,0:T(8,128)(2,1)} %latent_h.1, bf16[64,2048]{1,0:T(8,128)(2,1)} %context_h.1, bf16[256,512]{1,0:T(8,128)(2,1)} %shift_h.1, ...), custom_call_target="tpu_custom_call" | custom-call | tf_op jit(solution)/shard_map/pallas_call | solution.py:560
  102.7 3.2 %copy.19 = bf16[512,2048]{1,0:T(8,128)(2,1)} copy(bf16[512,2048]{1,0:T(8,128)(2,1)} %shard_map.145) | data formatting | bytes 4194304
  (1 shorter events, 0.0 us)

commit v2 on v1

--- a/solution.py
+++ b/solution.py
@@ -35,7 +35,12 @@
     return x * cosines + partner * sines
 
 
-def kernel(
+def kernel(sp_n, tp_n, small_n, *refs):
+    act = refs[1] if small_n == 2 else None
+    body(sp_n, tp_n, act, refs[0], *refs[small_n:])
+
+
+def body(
     sp_n,
     tp_n,
     act,
@@ -71,6 +76,7 @@
     heads_all,
     ow_all,
     acc,
+    gates,
     out_v,
     sc_send,
     sc_recv,
@@ -89,10 +95,16 @@
     slr,
     ins,
     inr,
+    wos,
+    wor,
     wys,
     wyr,
+    wxs,
+    wxr,
     wps,
     wpr,
+    wqs,
+    wqr,
     hys,
     hyr,
     hps,
@@ -111,6 +123,10 @@
     H = W // HEAD_DIM
     R = sl_send.shape[1]
     per = HEAD_DIM // R
+    CN = ow_h.shape[0]
+    half = CN // 2
+    parity = lax.rem(me, 2)
+    beside = me + 1 - 2 * parity
 
     loads = [
         pltpu.make_async_copy(src, dst, load_sem.at[i])
@@ -125,7 +141,7 @@
                 (wv_h, wbuf.at[2]),
                 (wq_h, wbuf.at[0]),
                 (wg_h, wbuf.at[3]),
-                (ow_h, ow_all.at[pl.ds(tp * H, H)]),
+                (ow_h, ow_all.at[pl.ds(tp * CN, CN)]),
             ]
         )
     ]
@@ -166,7 +182,12 @@
     def sp_copy(off, src, dst, ss, rs):
         return remote(src, dst, ss.at[off], rs.at[off], {"sp": lax.rem(me + off, sp_n)})
 
-    a = act[me].astype(F32)
+    MR = modw.shape[1]
+    if act is None:
+        a = gain[0:2, pl.ds(pl.multiple_of(me * MR, MR), MR)]
+        a = jnp.concatenate([a, jnp.zeros((6, MR), F32)], axis=0)
+    else:
+        a = act[me].astype(F32)
     activation = (a / (1.0 + jnp.exp(-a))).astype(BF16)
     for i in range(3):
         loads[i].wait()
@@ -184,35 +205,6 @@
 
     def y_source(off):
         return lax.rem(my_y - off + y_n, y_n) * 2 + core
-
-    def wy(off, c):
-        return remote(
-            ow_h.at[c],
-            ow_all.at[tp * H + c],
-            wys.at[off * H + c],
-            wyr.at[off * H + c],
-            y_peer(off),
-        )
-
-    def wp(off, c):
-        block = y_source(off) * H + c
-        return remote(
-            ow_all.at[block],
-            ow_all.at[block],
-            wps.at[off * H + c],
-            wpr.at[off * H + c],
-            {"tp": other},
-        )
-
-    for c in range(H):
-        each(y_n, lambda off: wy(off, c).start())
-
-    def relay_weight(c):
-        def one(off):
-            wy(off, c).wait_recv()
-            wp(off, c).start()
-
-        each(y_n, one)
 
     rows = 64
     loads[3].wait()
@@ -252,16 +244,6 @@
 
     each(tp_n, lambda off: m2(off).start())
     mod_all[tp] = mod_sum[...]
-    loads[9].wait()
-
-    def wown(c):
-        block = tp * H + c
-        return remote(
-            ow_all.at[block], ow_all.at[block], wps.at[c], wpr.at[c], {"tp": other}
-        )
-
-    for c in range(H):
-        wown(c).start()
 
     token = lax.broadcasted_iota(jnp.int32, (T, HEAD_DIM), 0)
     lane = lax.broadcasted_iota(jnp.int32, (T, HEAD_DIM), 1)
@@ -291,6 +273,62 @@
 
     each(tp_n, lambda off: m2(off).wait_recv())
 
+    def gate_row(b, carry):
+        gates[0:1, pl.ds(pl.multiple_of(b * W, W), W)] = mod_all[b, 4:5, :]
+        return carry
+
+    lax.fori_loop(0, tp_n, gate_row, 0)
+
+    wown = remote(ow_h, ow_all.at[pl.ds(tp * CN, CN)], wos.at[0], wor.at[0], {"tp": other})
+
+    def wy(off, i):
+        c = parity * half + i
+        return remote(
+            ow_h.at[c],
+            ow_all.at[tp * CN + c],
+            wys.at[off * half + i],
+            wyr.at[off * half + i],
+            y_peer(off),
+        )
+
+    def passed(off, i, side, ss, rs, where):
+        c = ow_all.at[y_source(off) * CN + side * half + i]
+        return remote(c, c, ss.at[off * half + i], rs.at[off * half + i], where)
+
+    def wx(off, i):
+        return passed(off, i, parity, wxs, wxr, {"sp": beside})
+
+    def wp(off, i):
+        return passed(off, i, parity, wps, wpr, {"tp": other})
+
+    def wq(off, i):
+        return passed(off, i, 1 - parity, wqs, wqr, {"tp": other})
+
+    for i in range(half):
+        each(y_n, lambda off: wy(off, i).start())
+    wown.start()
+
+    def relay_y(i):
+        def one(off):
+            wy(off, i).wait_recv()
+            wx(off, i).start()
+            wp(off, i).start()
+
+        each(y_n, one)
+
+    def relay_x(i):
+        def one(off):
+            wx(off, i).wait_recv()
+            wq(off, i).start()
+
+        each(y_n, one)
+
+    quarter = max(half // 4, 1)
+
+    def relay(which, phase):
+        for i in range(phase * quarter, min((phase + 1) * quarter, half)):
+            which(i)
+
     def modulate(source, base, row):
         height = min(rows, source.shape[0])
         tiles = source.shape[0] // height
@@ -300,10 +338,14 @@
             r = pl.multiple_of(lax.rem(i, tiles) * height, height)
             cols = pl.ds(pl.multiple_of(b * W, W), W)
             out_rows = pl.ds(pl.multiple_of(base + r, height), height)
-            x = source[pl.ds(r, height), cols].astype(F32) * inv[out_rows, 0:1]
-            x = x * gain[:, cols]
-            x = x * (1.0 + mod_all[b, 2 + row : 3 + row, :]) + mod_all[b, row : row + 1, :]
-            hid[out_rows, cols] = x.astype(BF16)
+            level = inv[out_rows, :]
+            lift = gain[gain.shape[0] - 1 :, cols] * (1.0 + mod_all[b, 2 + row : 3 + row, :])
+            shift = mod_all[b, row : row + 1, :]
+            x = source[pl.ds(r, height), cols].astype(F32)
+            for h in range(H):
+                c = slice(h * HEAD_DIM, (h + 1) * HEAD_DIM)
+                to = pl.ds(pl.multiple_of(b * W + h * HEAD_DIM, HEAD_DIM), HEAD_DIM)
+                hid[out_rows, to] = (x[:, c] * level * lift[:, c] + shift[:, c]).astype(BF16)
             return carry
 
         lax.fori_loop(0, tp_n * tiles, one, 0)
@@ -363,6 +405,7 @@
         proj[1, 0:T, cols] = k.astype(BF16)
 
     each(sp_n, lambda off: slcopy(off).start())
+    relay(relay_y, 0)
     sc_recv[me] = sc_send[me]
     sl_recv[me] = sl_send[me]
 
@@ -371,6 +414,7 @@
     loads[8].wait()
     project(3, T)
 
+    relay(relay_y, 1)
     each(sp_n, lambda off: scopy(off).wait_recv())
     each(sp_n, lambda off: slcopy(off).wait_recv())
     backward = (me * R) // (H * HEAD_DIM)
@@ -389,20 +433,24 @@
     lax.fori_loop(0, sp_n, scan, start)
     each(sp_n, lambda off: incopy(off).start())
     in_recv[me] = in_send[me]
-
+    relay(relay_y, 2)
+
+    st = 256 if T % 256 == 0 else mt
     for h in range(H):
         cols = slice(h * HEAD_DIM, (h + 1) * HEAD_DIM)
         q = rotated(proj[0, 0:T, cols].astype(F32), cosb[...], sinb[...], low).astype(BF16)
         proj[0, 0:T, cols] = q
 
         def score_rows(i, carry):
-            r = pl.ds(pl.multiple_of(i * mt, mt), mt)
+            r = pl.ds(pl.multiple_of(i * st, st), st)
             s = dot_columns(proj[0, r, cols], proj[1, 0:T, cols]) * mix[h, r, :].astype(F32)
             local[r, cols] = dot(s.astype(BF16), proj[2, 0:T, cols])
             return carry
 
-        lax.fori_loop(0, T // mt, score_rows, 0)
-
+        lax.fori_loop(0, T // st, score_rows, 0)
+
+    relay(relay_y, 3)
+    relay(relay_x, 0)
     each(sp_n, lambda off: incopy(off).wait_recv())
 
     def hview(block, h):
@@ -444,82 +492,92 @@
         each(y_n, lambda off: hy(off, h).start())
         hown(h).start()
 
-    for c in range(H):
-        relay_weight(c)
-
-    ot = 256
-
-    def block_product(block, first, last):
+    relay(relay_x, 1)
+
+    ot = min(256, W)
+
+    def out_tile(j):
+        cols = pl.ds(pl.multiple_of(j * ot, ot), ot)
+        return pltpu.make_async_copy(out_v.at[:, cols], out_h.at[:, cols], out_sem.at[j])
+
+    def block_product(block, first=False, last=False):
         def one(j, carry):
             cols = pl.ds(pl.multiple_of(j * ot, ot), ot)
-            value = None
-            for c in range(0, H, 2 if H % 2 == 0 else 1):
-                width = 2 if H % 2 == 0 else 1
-                piece = heads_all[block, :, c * HEAD_DIM : (c + width) * HEAD_DIM]
-                weight = ow_all[pl.ds(block * H + c, width), :, cols].reshape(
-                    width * HEAD_DIM, ot
-                )
-                term = dot(piece, weight)
-                value = term if value is None else value + term
+            weight = ow_all[pl.ds(block * CN, CN), :, cols].reshape(W, ot)
+            value = dot(heads_all[block], weight)
             if not first:
                 value = value + acc[:, cols]
-            acc[:, cols] = value
+            if last:
+                value = lat[:, cols].astype(F32) + gates[0:1, cols] * value
+                out_v[:, cols] = value.astype(BF16)
+                out_tile(j).start()
+            else:
+                acc[:, cols] = value
             return carry
 
         lax.fori_loop(0, D // ot, one, 0)
 
-    block_product(tp, True, False)
+    loads[9].wait()
+    block_product(tp, first=True)
     for h in range(H):
         hown(h).wait_recv()
-        wown(h).wait_recv()
-    block_product(other, False, False)
+    wown.wait_recv()
+    relay(relay_x, 2)
+    block_product(other)
+    relay(relay_x, 3)
 
     def far(off):
         for h in range(H):
             hy(off, h).wait_recv()
             hp(off, h).start()
-        block_product(y_source(off), False, False)
+        block_product(y_source(off))
 
     each(y_n, far)
 
     def farther(off):
         for h in range(H):
             hp(off, h).wait_recv()
-            wp(off, h).wait_recv()
-        block_product(lax.rem(my_y - off + y_n, y_n) * 2 + 1 - core, False, False)
-
-    each(y_n, farther)
-
-    def finish(i, carry):
-        b = i // (T // rows)
-        r = pl.multiple_of(lax.rem(i, T // rows) * rows, rows)
-        cols = pl.ds(pl.multiple_of(b * W, W), W)
-        value = lat[pl.ds(r, rows), cols].astype(F32) + mod_all[b, 4:5, :] * acc[pl.ds(r, rows), cols]
-        out_v[pl.ds(r, rows), cols] = value.astype(BF16)
-        return carry
-
-    lax.fori_loop(0, tp_n * (T // rows), finish, 0)
-    result = pltpu.make_async_copy(out_v, out_h, out_sem)
-    result.start()
+        for i in range(half):
+            wp(off, i).wait_recv()
+            wq(off, i).wait_recv()
+
+    def farther_block(off):
+        return y_source(off) + 1 - 2 * core
+
+    def middle(off):
+        farther(off)
+        block_product(farther_block(off))
+
+    each(y_n - 1, middle)
+    farther(y_n - 1)
+    block_product(farther_block(y_n - 1), last=True)
 
     each(sp_n, lambda off: m1(off).wait_send())
     each(tp_n, lambda off: m2(off).wait_send())
     each(sp_n, lambda off: scopy(off).wait_send())
     each(sp_n, lambda off: slcopy(off).wait_send())
     each(sp_n, lambda off: incopy(off).wait_send())
+    wown.wait_send()
     for h in range(H):
-        wown(h).wait_send()
         hown(h).wait_send()
 
     def settle(off):
+        for i in range(half):
+            wy(off, i).wait_send()
+            wx(off, i).wait_send()
+            wp(off, i).wait_send()
+            wq(off, i).wait_send()
         for h in range(H):
-            wy(off, h).wait_send()
-            wp(off, h).wait_send()
             hy(off, h).wait_send()
             hp(off, h).wait_send()
 
     each(y_n, settle)
-    result.wait()
+
+    def written(j, carry):
+        out_tile(j).wait()
+        return carry
+
+    lax.fori_loop(0, D // ot, written, 0)
 
 
 def local_program(
@@ -546,10 +604,15 @@
     MR, W = shift_weight.shape
     H = W // HEAD_DIM
     R = 2 * H * HEAD_DIM // sp_n
-    pair = jnp.stack([condition, context_condition]).reshape(2, sp_n, MR)
-    act = jnp.pad(jnp.transpose(pair, (1, 0, 2)), ((0, 0), (0, 14), (0, 0)))
-    gain = norm_gain.astype(F32).reshape(1, D)
-    ow = out_weight.reshape(H, HEAD_DIM, D)
+    CN = W // 64
+    ow = out_weight.reshape(CN, W // CN, D)
+    if MR % HEAD_DIM == 0:
+        rows = jnp.concatenate([condition, context_condition, norm_gain])
+        small = [rows.astype(F32).reshape(3, D)]
+    else:
+        pair = jnp.stack([condition, context_condition]).reshape(2, sp_n, MR)
+        act = jnp.pad(jnp.transpose(pair, (1, 0, 2)), ((0, 0), (0, 14), (0, 0)))
+        small = [norm_gain.astype(F32).reshape(1, D), act]
     y_n = tp_n // 2
     vm = pl.BlockSpec(memory_space=pltpu.VMEM)
     sm = pl.BlockSpec(memory_space=pltpu.SMEM)
@@ -558,9 +621,9 @@
     dma = pltpu.SemaphoreType.DMA
     state = V((sp_n, R, HEAD_DIM), BF16)
     return pl.pallas_call(
-        functools.partial(kernel, sp_n, tp_n),
+        functools.partial(kernel, sp_n, tp_n, len(small)),
         out_shape=jax.ShapeDtypeStruct((T, D), BF16),
-        in_specs=[vm, vm, sm, sm] + [hb] * 10,
+        in_specs=[vm] * len(small) + [sm, sm] + [hb] * 10,
         out_specs=hb,
         scratch_shapes=[
             V((T, D), BF16),
@@ -579,8 +642,9 @@
             V((H, T, T), BF16),
             V((T, W), F32),
             V((tp_n, T, W), BF16),
-            V((tp_n * H, HEAD_DIM, D), BF16),
+            V((tp_n * CN, W // CN, D), BF16),
             V((T, D), F32),
+            V((8, D), F32),
             V((T, D), BF16),
             state,
             state,
@@ -595,14 +659,15 @@
             dma((tp_n,)),
         ]
         + [dma((sp_n,))] * 6
-        + [dma((y_n * H,))] * 8
-        + [dma],
+        + [dma((1,))] * 2
+        + [dma((y_n * CN // 2,))] * 8
+        + [dma((y_n * H,))] * 4
+        + [dma((D // min(256, W),))],
         compiler_params=pltpu.CompilerParams(
             collective_id=0, has_side_effects=True, vmem_limit_bytes=60 * 1024 * 1024
         ),
     )(
-        act,
-        gain,
+        *small,
         forward_decay,
         backward_decay,
         latent,

time: 106 us -> 65.1 us (0.61)
  Pallas kernels: 99.3 us -> 60.3 us
  local copies, waits for them, and re-layouts: 5.19 us -> 3.79 us
    pallas_call x1, Pallas kernels: 99.3 us -> 60.3 us  [local_program(): pl.pallas_call(functools.partial(kernel, sp_n, tp_n, len(small)), out_sha...]
    another operation x2 -> x0, local copies, waits for them, and re-layouts: 1.39 us -> none  [local_program(): pair = jnp.stack([condition, context_condition]).reshape(2, sp_n, MR)]
    reshape x1 -> x0, other arithmetic: 1.28 us -> none  [local_program(): gain = norm_gain.astype(F32).reshape(1, D)]
where the time goes in v2:
time: 65.1 us; the launch traced here: 64.8 us
  Pallas kernels  60.3 us (93%)
  local copies, waits for them, and re-layouts  3.79 us (6%)
  other arithmetic  0.72 us (1%)
    pallas_call x1, Pallas kernels, local_program(): pl.pallas_call(functools.partial(kernel, sp_n, tp_n, len(small)), out_sha...  60.3 us
    unnamed x1, local copies, waits for them, and re-layouts  3.16 us

profile of v2, /device:TPU:0, one launch (start us, length us, event | category | flops | bytes accessed | tf_op | source)
XLA Modules:
  0.0 64.8 jit_solution(9856343378336401042)
XLA Ops:
  0.0 0.7 %maximum_convert_fusion = f32[6144]{0:T(1024)S(1)} fusion(bf16[2048]{0:T(1024)(128)(2,1)} %param.22, bf16[2048]{0:T(1024)(128)(2,1)} %param.18, bf16[2048]{0:T(1024)(128)(2,1)} %param.17), kind=kLoop, calls=%fused_computation | loop fusion | flops 36864 | bytes 36864 | tf_op jit(solution)/shard_map/convert_element_type | solution.py:611
  0.7 0.6 reshape.8.refs_0_
  1.4 60.3 %shard_map.145 = bf16[512,2048]{1,0:T(8,128)(2,1)} custom-call(f32[3,2048]{1,0:T(4,128)} %reshape.8.refs_0_, f32[4]{0:T(128)} %refs_1_.1, f32[4]{0:T(128)} %refs_2_.1, bf16[512,2048]{1,0:T(8,128)(2,1)} %refs_3_.1, bf16[64,2048]{1,0:T(8,128)(2,1)} %refs_4_.1, bf16[256,512]{1,0:T(8,128)(2,1)} %refs_5_.1, bf16[256,512]{1,0:T(8,128)(2,1)} %refs_6_.1, ...), custom_call_target="tpu_custom_call" | custom-call | tf_op jit(solution)/shard_map/pallas_call | solution.py:623
  61.7 3.2 %copy.17 = bf16[512,2048]{1,0:T(8,128)(2,1)} copy(bf16[512,2048]{1,0:T(8,128)(2,1)} %shard_map.145) | data formatting | bytes 4194304

commit v3 on v2

--- a/solution.py
+++ b/solution.py
@@ -350,23 +350,23 @@
 
         lax.fori_loop(0, tp_n * tiles, one, 0)
 
-    modulate(lat, 0, 0)
     modulate(ctx, T, 1)
 
     nt = min(256, W)
 
-    def project(index, height):
+    def project(index, base, height):
         def one(j, carry):
             cols = pl.ds(pl.multiple_of(j * nt, nt), nt)
-            proj[index, 0:height, cols] = dot(hid[0:height, :], wbuf[index, :, cols]).astype(BF16)
+            product = dot(hid[base : base + height, :], wbuf[index, :, cols])
+            proj[index, base : base + height, cols] = product.astype(BF16)
             return carry
 
         lax.fori_loop(0, W // nt, one, 0)
 
     loads[5].wait()
-    project(1, T + CR)
     loads[6].wait()
-    project(2, T + CR)
+    project(1, T, CR)
+    project(2, T, CR)
 
     scale = HEAD_DIM**-0.5
     step = token.astype(F32)
@@ -395,6 +395,10 @@
         return sp_copy(off, in_send.at[lax.rem(me + off, sp_n)], in_recv.at[me], ins, inr)
 
     each(sp_n, lambda off: scopy(off).start())
+
+    modulate(lat, 0, 0)
+    project(1, 0, T)
+    project(2, 0, T)
 
     for h in range(H):
         cols = slice(h * HEAD_DIM, (h + 1) * HEAD_DIM)
@@ -410,9 +414,9 @@
     sl_recv[me] = sl_send[me]
 
     loads[7].wait()
-    project(0, T)
+    project(0, 0, T)
     loads[8].wait()
-    project(3, T)
+    project(3, 0, T)
 
     relay(relay_y, 1)
     each(sp_n, lambda off: scopy(off).wait_recv())
@@ -500,11 +504,20 @@
         cols = pl.ds(pl.multiple_of(j * ot, ot), ot)
         return pltpu.make_async_copy(out_v.at[:, cols], out_h.at[:, cols], out_sem.at[j])
 
-    def block_product(block, first=False, last=False):
+    rows_each = HEAD_DIM * CN // W
+
+    def product(blocks, low_head, high_head, first=False, last=False):
+        k = slice(low_head * HEAD_DIM, high_head * HEAD_DIM)
+        count = (high_head - low_head) * rows_each
+
         def one(j, carry):
             cols = pl.ds(pl.multiple_of(j * ot, ot), ot)
-            weight = ow_all[pl.ds(block * CN, CN), :, cols].reshape(W, ot)
-            value = dot(heads_all[block], weight)
+            value = None
+            for block in blocks:
+                chunk = pl.ds(block * CN + low_head * rows_each, count)
+                weight = ow_all[chunk, :, cols].reshape((high_head - low_head) * HEAD_DIM, ot)
+                term = dot(heads_all[block, :, k], weight)
+                value = term if value is None else value + term
             if not first:
                 value = value + acc[:, cols]
             if last:
@@ -518,39 +531,35 @@
         lax.fori_loop(0, D // ot, one, 0)
 
     loads[9].wait()
-    block_product(tp, first=True)
     for h in range(H):
         hown(h).wait_recv()
     wown.wait_recv()
     relay(relay_x, 2)
-    block_product(other)
+    product([tp, other], 0, H, first=True)
     relay(relay_x, 3)
-
-    def far(off):
-        for h in range(H):
+    groups = [(0, H // 2), (H // 2, H)] if H > 1 else [(0, 1)]
+
+    def far_step(off, group, last):
+        low_head, high_head = groups[group]
+        for h in range(low_head, high_head):
             hy(off, h).wait_recv()
             hp(off, h).start()
-        block_product(y_source(off))
-
-    each(y_n, far)
-
-    def farther(off):
-        for h in range(H):
+        for h in range(low_head, high_head):
             hp(off, h).wait_recv()
-        for i in range(half):
-            wp(off, i).wait_recv()
-            wq(off, i).wait_recv()
-
-    def farther_block(off):
-        return y_source(off) + 1 - 2 * core
+        if group == 0:
+            for i in range(half):
+                wp(off, i).wait_recv()
+                wq(off, i).wait_recv()
+        block = y_source(off)
+        product([block, block + 1 - 2 * core], low_head, high_head, last=last)
 
     def middle(off):
-        farther(off)
-        block_product(farther_block(off))
+        for group in range(len(groups)):
+            far_step(off, group, False)
 
     each(y_n - 1, middle)
-    farther(y_n - 1)
-    block_product(farther_block(y_n - 1), last=True)
+    for group in range(len(groups)):
+        far_step(y_n - 1, group, group == len(groups) - 1)
 
     each(sp_n, lambda off: m1(off).wait_send())
     each(tp_n, lambda off: m2(off).wait_send())

time: 65.1 us -> 66.3 us (1.018)
  Pallas kernels: 60.3 us -> 61.5 us
    pallas_call x1, Pallas kernels: 60.3 us -> 61.5 us  [local_program(): pl.pallas_call(functools.partial(kernel, sp_n, tp_n, len(small)), out_sha...]
where the time goes in v3:
time: 66.3 us; the launch traced here: 66 us
  Pallas kernels  61.5 us (93%)
  local copies, waits for them, and re-layouts  3.79 us (6%)
  other arithmetic  0.72 us (1%)
    pallas_call x1, Pallas kernels, local_program(): pl.pallas_call(functools.partial(kernel, sp_n, tp_n, len(small)), out_sha...  61.5 us
    unnamed x1, local copies, waits for them, and re-layouts  3.16 us

profile of v3, /device:TPU:0, one launch (start us, length us, event | category | flops | bytes accessed | tf_op | source)
XLA Modules:
  0.0 66.0 jit_solution(10312374444210542665)
XLA Ops:
  0.0 0.7 %maximum_convert_fusion = f32[6144]{0:T(1024)S(1)} fusion(bf16[2048]{0:T(1024)(128)(2,1)} %param.22, bf16[2048]{0:T(1024)(128)(2,1)} %param.18, bf16[2048]{0:T(1024)(128)(2,1)} %param.17), kind=kLoop, calls=%fused_computation | loop fusion | flops 36864 | bytes 36864 | tf_op jit(solution)/shard_map/convert_element_type | solution.py:620
  0.7 0.6 reshape.8.refs_0_
  1.4 61.5 %shard_map.145 = bf16[512,2048]{1,0:T(8,128)(2,1)} custom-call(f32[3,2048]{1,0:T(4,128)} %reshape.8.refs_0_, f32[4]{0:T(128)} %refs_1_.1, f32[4]{0:T(128)} %refs_2_.1, bf16[512,2048]{1,0:T(8,128)(2,1)} %refs_3_.1, bf16[64,2048]{1,0:T(8,128)(2,1)} %refs_4_.1, bf16[256,512]{1,0:T(8,128)(2,1)} %refs_5_.1, bf16[256,512]{1,0:T(8,128)(2,1)} %refs_6_.1, ...), custom_call_target="tpu_custom_call" | custom-call | tf_op jit(solution)/shard_map/pallas_call | solution.py:632
  62.9 3.2 %copy.17 = bf16[512,2048]{1,0:T(8,128)(2,1)} copy(bf16[512,2048]{1,0:T(8,128)(2,1)} %shard_map.145) | data formatting | bytes 4194304

commit v4 on v3

--- a/solution.py
+++ b/solution.py
@@ -206,6 +206,18 @@
     def y_source(off):
         return lax.rem(my_y - off + y_n, y_n) * 2 + core
 
+    def wy(off, i):
+        c = parity * half + i
+        return remote(
+            ow_h.at[c],
+            ow_all.at[tp * CN + c],
+            wys.at[off * half + i],
+            wyr.at[off * half + i],
+            y_peer(off),
+        )
+
+    each(y_n, lambda off: wy(off, 0).start())
+
     rows = 64
     loads[3].wait()
     loads[4].wait()
@@ -281,16 +293,6 @@
 
     wown = remote(ow_h, ow_all.at[pl.ds(tp * CN, CN)], wos.at[0], wor.at[0], {"tp": other})
 
-    def wy(off, i):
-        c = parity * half + i
-        return remote(
-            ow_h.at[c],
-            ow_all.at[tp * CN + c],
-            wys.at[off * half + i],
-            wyr.at[off * half + i],
-            y_peer(off),
-        )
-
     def passed(off, i, side, ss, rs, where):
         c = ow_all.at[y_source(off) * CN + side * half + i]
         return remote(c, c, ss.at[off * half + i], rs.at[off * half + i], where)
@@ -304,7 +306,7 @@
     def wq(off, i):
         return passed(off, i, 1 - parity, wqs, wqr, {"tp": other})
 
-    for i in range(half):
+    for i in range(1, half):
         each(y_n, lambda off: wy(off, i).start())
     wown.start()
 
@@ -350,6 +352,7 @@
 
         lax.fori_loop(0, tp_n * tiles, one, 0)
 
+    relay(relay_y, 0)
     modulate(ctx, T, 1)
 
     nt = min(256, W)
@@ -409,7 +412,7 @@
         proj[1, 0:T, cols] = k.astype(BF16)
 
     each(sp_n, lambda off: slcopy(off).start())
-    relay(relay_y, 0)
+    relay(relay_y, 1)
     sc_recv[me] = sc_send[me]
     sl_recv[me] = sl_send[me]
 
@@ -418,7 +421,6 @@
     loads[8].wait()
     project(3, 0, T)
 
-    relay(relay_y, 1)
     each(sp_n, lambda off: scopy(off).wait_recv())
     each(sp_n, lambda off: slcopy(off).wait_recv())
     backward = (me * R) // (H * HEAD_DIM)

time: 66.3 us -> 62.7 us (0.946)
  Pallas kernels: 61.5 us -> 58 us
    pallas_call x1, Pallas kernels: 61.5 us -> 58 us  [local_program(): pl.pallas_call(functools.partial(kernel, sp_n, tp_n, len(small)), out_sha...]
where the time goes in v4:
time: 62.7 us; the launch traced here: 62.5 us
  Pallas kernels  58 us (93%)
  local copies, waits for them, and re-layouts  3.79 us (6%)
  other arithmetic  0.72 us (1%)
    pallas_call x1, Pallas kernels, local_program(): pl.pallas_call(functools.partial(kernel, sp_n, tp_n, len(small)), out_sha...  58 us
    unnamed x1, local copies, waits for them, and re-layouts  3.16 us

profile of v4, /device:TPU:0, one launch (start us, length us, event | category | flops | bytes accessed | tf_op | source)
XLA Modules:
  0.0 62.5 jit_solution(8982212301195847394)
XLA Ops:
  0.0 0.7 %maximum_convert_fusion = f32[6144]{0:T(1024)S(1)} fusion(bf16[2048]{0:T(1024)(128)(2,1)} %param.22, bf16[2048]{0:T(1024)(128)(2,1)} %param.18, bf16[2048]{0:T(1024)(128)(2,1)} %param.17), kind=kLoop, calls=%fused_computation | loop fusion | flops 36864 | bytes 36864 | tf_op jit(solution)/shard_map/convert_element_type | solution.py:622
  0.7 0.6 %reshape.8.refs_0_ = f32[3,2048]{1,0:T(4,128)} reshape(f32[6144]{0:T(1024)S(1)} %maximum_convert_fusion) | data formatting | bytes 49152 | tf_op jit(solution)/shard_map/convert_element_type | solution.py:622
  1.4 58.0 %shard_map.145 = bf16[512,2048]{1,0:T(8,128)(2,1)} custom-call(f32[3,2048]{1,0:T(4,128)} %reshape.8.refs_0_, f32[4]{0:T(128)} %refs_1_.1, f32[4]{0:T(128)} %refs_2_.1, bf16[512,2048]{1,0:T(8,128)(2,1)} %refs_3_.1, bf16[64,2048]{1,0:T(8,128)(2,1)} %refs_4_.1, bf16[256,512]{1,0:T(8,128)(2,1)} %refs_5_.1, bf16[256,512]{1,0:T(8,128)(2,1)} %refs_6_.1, ...), custom_call_target="tpu_custom_call" | custom-call | tf_op jit(solution)/shard_map/pallas_call | solution.py:634
  59.3 3.2 %copy.17 = bf16[512,2048]{1,0:T(8,128)(2,1)} copy(bf16[512,2048]{1,0:T(8,128)(2,1)} %shard_map.145) | data formatting | bytes 4194304
